TPU v7x, 32 devices: a whole 2x2x4 slice. The times are simulated.
32 devices in a mesh: fs: 16 (over z, y, x), tp: 2 (over core).
Axes of the slice: x: 2, y: 2, z: 4, core: 2. Of those that a mesh axis runs over, the one named last changes fastest.
Arguments:
- prompt: bfloat16 [5120, 2048], P('fs', 'tp'), may hold values from -6 to 6
- norm_gain: float32 [2048], P('fs'), may hold values from 0.1 to 1.9
- gate_master: float32 [2048, 3072], P('fs', 'tp'), may hold values from -0.125 to 0.125
- up_master: float32 [2048, 3072], P('fs', 'tp'), may hold values from -0.125 to 0.125
- down_master: float32 [2048, 3072], P('fs', 'tp'), may hold values from -0.109375 to 0.109375
Outputs:
- gate_new: bfloat16 [3072, 2048], P('tp')
- up_new: bfloat16 [3072, 2048], P('tp')
- down_new: bfloat16 [3072, 2048], P('tp')
- mixed: bfloat16 [2048, 5120], P('tp', 'fs')
All inputs are finite; a program needn't handle non-finite values.
Results may differ from a plain program's by a relative error of at most 0.0082.
Values may be sent and summed in bfloat16 or wider, within the bound.
A program may use at most 128 MiB of HBM per device.

v0:
```python
import jax
import jax.numpy as jnp
from jax import lax
from jax.sharding import PartitionSpec as P


def on_device(prompt, norm_gain, gate_master, up_master, down_master):
    gain_col = norm_gain[:, None]
    gate_low = (gate_master * gain_col).astype(jnp.bfloat16).T
    up_low = (up_master * gain_col).astype(jnp.bfloat16).T
    down_low = down_master.astype(jnp.bfloat16).T
    whole = lax.all_gather(prompt, "tp", axis=1, tiled=True)
    values = whole.astype(jnp.float32)
    normed = (values * lax.rsqrt(jnp.mean(values * values, axis=1, keepdims=True) + 1e-06)).astype(
        jnp.bfloat16
    )
    contract = (((1,), (1,)), ((), ()))
    gate_new, up_new, down_new = (
        lax.all_gather(gate_low, "fs", axis=1, tiled=True),
        lax.all_gather(up_low, "fs", axis=1, tiled=True),
        lax.all_gather(down_low, "fs", axis=1, tiled=True),
    )
    gate = lax.dot_general(normed, gate_new, contract, preferred_element_type=jnp.float32)
    up = lax.dot_general(normed, up_new, contract, preferred_element_type=jnp.float32)
    hidden = (jax.nn.silu(gate) * up).astype(jnp.bfloat16)
    mixed = lax.psum_scatter(
        lax.dot_general(
            down_new, hidden, (((0,), (1,)), ((), ())), preferred_element_type=jnp.float32
        ),
        "tp",
        scatter_dimension=0,
        tiled=True,
    )
    return (gate_new, up_new, down_new, mixed.astype(jnp.bfloat16))


def solution(mesh):
    placed = (P("fs", "tp"), P("fs"), P("fs", "tp"), P("fs", "tp"), P("fs", "tp"))
    return jax.shard_map(
        on_device,
        mesh=mesh,
        in_specs=placed,
        out_specs=(P("tp", None), P("tp", None), P("tp", None), P("tp", "fs")),
        check_vma=False,
    )
```

profile of v0, /device:TPU:0, one launch (start us, length us, event | category | flops | bytes accessed | tf_op | source)
XLA Modules:
  0.0 414.9 jit_solution(16847187545937609317)
XLA Ops:
  7.2 0.0 copy-start.1
  7.2 0.0 copy-start.3
  7.2 0.0 all-gather.11.cloned.1.call-start
  7.2 0.7 all-gather.11.cloned.1.call-update
  7.9 0.0 all-gather.5.cloned.1.call-start
  8.0 1.4 copy.10
  9.4 0.0 copy-done.1
  9.4 0.0 copy-start.2
  9.4 0.3 copy.9
  9.7 0.0 copy-done.3
  9.7 1.0 fusion.8
  10.7 0.0 all-gather.5.cloned.1.call-update
  10.7 0.0 all-gather.7.cloned.1.call-start
  10.7 0.7 all-gather.7.cloned.1.call-update
  11.4 0.0 all-gather.9.cloned.1.call-start
  11.5 0.0 copy-done.2
  11.5 0.9 copy.11
  12.4 0.0 all-gather.9.cloned.1.call-update
  12.4 0.0 reduce-scatter.2.cloned.1.call-start
  12.5 9.2 %all-gather.11.cloned.1.call-done = bf16[320,2048]{1,0:T(8,128)(2,1)} async-done(((bf16[320,1024]{1,0:T(8,128)(2,1)}), bf16[320,2048]{1,0:T(8,128)(2,1)}) %all-gather.11.cloned.1.call-update) | async-done | bytes 1310736 | tf_op jit(solution)/shard_map/all_gather | solution.py:12
  21.7 1.7 fusion.1
  23.4 0.0 copy-start
  23.4 117.8 %all-gather.5.cloned.1.call-done = bf16[1536,2048]{1,0:T(8,128)(2,1)} async-done(((bf16[1536,128]{1,0:T(8,128)(2,1)}), bf16[1536,2048]{1,0:T(8,128)(2,1)}) %all-gather.5.cloned.1.call-update) | async-done | bytes 6291472 | tf_op jit(solution)/shard_map/all_gather | solution.py:19
  141.2 5.4 %fusion.5 = f32[320,1536]{1,0:T(8,128)S(1)} fusion(bf16[1536,2048]{1,0:T(8,128)(2,1)} %all-gather.5.cloned.1.call-done, bf16[320,2048]{1,0:T(8,128)(2,1)} %all-gather.11.cloned.1.call-done, f32[320]{0:T(512)S(1)} %add_rsqrt_fusion), kind=kOutput, calls=%fused_computation.9 | convolution fusion | flops 2015232000 | bytes 9569536 | tf_op jit(solution)/shard_map/dot_general | solution.py:23
  146.6 111.1 %all-gather.7.cloned.1.call-done = bf16[1536,2048]{1,0:T(8,128)(2,1)} async-done(((bf16[1536,128]{1,0:T(8,128)(2,1)}), bf16[1536,2048]{1,0:T(8,128)(2,1)}) %all-gather.7.cloned.1.call-update) | async-done | bytes 6291472 | tf_op jit(solution)/shard_map/all_gather | solution.py:20
  257.7 116.4 %all-gather.9.cloned.1.call-done = bf16[1536,2048]{1,0:T(8,128)(2,1)} async-done(((bf16[1536,128]{1,0:T(8,128)(2,1)}), bf16[1536,2048]{1,0:T(8,128)(2,1)}) %all-gather.9.cloned.1.call-update) | async-done | bytes 6291472 | tf_op jit(solution)/shard_map/all_gather | solution.py:21
  374.1 0.0 copy-done
  374.1 10.6 %convolution_bitcast_fusion = f32[2048,320]{0,1:T(8,128)} fusion(bf16[1536,2048]{1,0:T(8,128)(2,1)} %all-gather.9.cloned.1.call-done, bf16[1536,2048]{1,0:T(8,128)(2,1)} %all-gather.7.cloned.1.call-done, f32[320,1536]{1,0:T(8,128)S(1)} %fusion.5, bf16[320,2048]{1,0:T(8,128)(2,1)S(1)} %copy-done, f32[320]{0:T(512)S(1)} %add_rsqrt_fusion), kind=kOutput, calls=%fused_computation.3 | convolution fusion | flops 4031447040 | bytes 18482432 | tf_op jit(solution)/shard_map/dot_general | solution.py:27
  384.7 0.0 reduce-scatter.2.cloned.1.call-update
  384.7 8.7 %reduce-scatter.2.cloned.1.call-done = f32[1024,320]{0,1:T(8,128)} async-done(((f32[2048,320]{0,1:T(8,128)}), f32[1024,320]{0,1:T(8,128)}) %reduce-scatter.2.cloned.1.call-update) | async-done | bytes 1310736 | tf_op jit(solution)/shard_map/reduce_scatter | solution.py:26
  393.4 0.0 slice-start
  393.4 2.4 convert_element_type.27
  395.8 0.0 slice-start.1
  395.8 0.0 slice-start.2
  395.8 6.8 %copy.15 = bf16[1536,2048]{1,0:T(8,128)(2,1)} copy(bf16[1536,2048]{1,0:T(8,128)(2,1)} %all-gather.5.cloned.1.call-done) | data formatting | bytes 12582912
  402.6 0.0 slice-done
  402.6 0.0 slice-done.1
  402.6 0.0 slice-start.3
  402.6 2.8 copy.16
  405.4 0.0 slice-done.2
  405.4 0.3 slice-done.3
  405.7 2.7 copy.17
  (3 shorter events, 0.0 us)
Async XLA Ops:
  7.2 2.2 copy-start.1
  7.2 2.5 copy-start.3
  7.2 14.5 %all-gather.11.cloned.1.call-start = ((), (), s32[]{:S(2)}) async-start(), calls=%async_computation.4 | async-start | bytes 1966080 | tf_op jit(solution)/shard_map/all_gather | solution.py:12
  7.9 133.3 %all-gather.5.cloned.1.call-start = ((), (), s32[]{:S(2)}) async-start(), calls=%async_computation.1 | async-start | bytes 6684672 | tf_op jit(solution)/shard_map/all_gather | solution.py:19
  9.4 2.1 copy-start.2
  10.7 247.0 %all-gather.7.cloned.1.call-start = ((), (), s32[]{:S(2)}) async-start(), calls=%async_computation.2 | async-start | bytes 6684672 | tf_op jit(solution)/shard_map/all_gather | solution.py:20
  11.4 362.7 %all-gather.9.cloned.1.call-start = ((), (), s32[]{:S(2)}) async-start(), calls=%async_computation.3 | async-start | bytes 6684672 | tf_op jit(solution)/shard_map/all_gather | solution.py:21
  12.4 381.0 %reduce-scatter.2.cloned.1.call-start = ((), (), s32[]{:S(2)}) async-start(), calls=%async_computation.5 | async-start | bytes 3932160 | tf_op jit(solution)/shard_map/reduce_scatter | solution.py:26
  23.4 350.7 %copy-start = (bf16[320,2048]{1,0:T(8,128)(2,1)S(1)}, bf16[320,2048]{1,0:T(8,128)(2,1)}, u32[]{:S(2)}) copy-start(bf16[320,2048]{1,0:T(8,128)(2,1)} %all-gather.11.cloned.1.call-done) | copy-start | bytes 3932164
  393.4 9.2 %slice-start = ((s8[6291456]{0:T(1024)(128)(4,1)}), s8[4194304]{0:T(1024)(128)(4,1)S(1)}, s32[]{:S(2)}) async-start(s8[6291456]{0:T(1024)(128)(4,1)} %bitcast.12), calls=%async_computation.6 | async-start | bytes 8388608
  395.8 6.8 %slice-start.1 = ((s8[6291456]{0:T(1024)(128)(4,1)}), s8[2097152]{0:T(1024)(128)(4,1)S(1)}, s32[]{:S(2)}) async-start(s8[6291456]{0:T(1024)(128)(4,1)} %bitcast.12), calls=%async_computation.7 | async-start | bytes 4194304
  395.8 9.6 %slice-start.2 = ((s8[6291456]{0:T(1024)(128)(4,1)}), s8[4194304]{0:T(1024)(128)(4,1)S(1)}, s32[]{:S(2)}) async-start(s8[6291456]{0:T(1024)(128)(4,1)} %bitcast.14), calls=%async_computation.8 | async-start | bytes 8388608
  402.6 3.1 slice-start.3
Sparse Core Ops, SparseCore 0:
  9.5 12.1 all-gather.10
  25.0 116.1 all-gather.4
  144.5 113.1 all-gather.6
  260.9 113.1 all-gather.8
  384.9 8.4 reduce-scatter.1
where the time goes:
time: 415 us
  waiting for transfers between devices  365 us (88%)
  matrix products  16 us (4%)
  local copies, waits for them, and re-layouts  15.2 us (4%)
  between operations  13.9 us (3%)
  other arithmetic  5.08 us (1%)
    all_gather x1, waiting for transfers between devices, on_device(): lax.all_gather(gate_low, 'fs', axis=1, tiled=True)  118 us
    all_gather x1, waiting for transfers between devices, on_device(): lax.all_gather(down_low, 'fs', axis=1, tiled=True)  116 us
    all_gather x1, waiting for transfers between devices, on_device(): lax.all_gather(up_low, 'fs', axis=1, tiled=True)  111 us
    unnamed x22, local copies, waits for them, and re-layouts  15.2 us
    dot_general x1, matrix products, on_device(): lax.dot_general(down_new, hidden, (((0,), (1,)), ((), ())), preferred_ele...  10.6 us
    all_gather x1, waiting for transfers between devices, on_device(): whole = lax.all_gather(prompt, 'tp', axis=1, tiled=True)  9.23 us
    reduce_scatter x1, waiting for transfers between devices, on_device(): lax.psum_scatter(lax.dot_general(down_new, hidden, (((0,), (1,)), ((), ()...  8.65 us
  transfers between devices with their start and end apart: 5, of which 5 were waited for; matrix products, arithmetic and copies ran while one was open for 3% of the time, Pallas kernels for 0%

commit v1 on v0

--- a/solution.py
+++ b/solution.py
@@ -1,14 +1,309 @@
+import functools
+
 import jax
 import jax.numpy as jnp
 from jax import lax
+from jax.experimental import pallas as pl
+from jax.experimental.pallas import tpu as pltpu
 from jax.sharding import PartitionSpec as P
 
-
-def on_device(prompt, norm_gain, gate_master, up_master, down_master):
+MESH = pl.DeviceIdType.MESH
+LANES = 128
+GATE, UP, DOWN = 0, 1, 2
+Z_UP, Z_DOWN, ALONG_A, ALONG_B = 0, 1, 2, 3
+CHUNKS = 2
+
+
+def gather_kernel(depth, low_refs, prompt_ref, full_refs, both_ref, send_sem, recv_sem, own_sem, pair_sem):
+    fs, tp = lax.axis_index("fs"), lax.axis_index("tp")
+    z, y, x = fs // 4, lax.rem(fs // 2, 2), lax.rem(fs, 2)
+    at_a, at_b = x * (1 - tp) + y * tp, y * (1 - tp) + x * tp
+    to_a, to_b = (1 - 2 * at_a) * (1 + tp), (1 - 2 * at_b) * (2 - tp)
+    peers = {Z_UP: fs + 4, Z_DOWN: fs - 4, ALONG_A: fs + to_a, ALONG_B: fs + to_b}
+    exists = {Z_UP: z + 1 < depth, Z_DOWN: z > 0, ALONG_A: None, ALONG_B: None}
+    rows = low_refs[0].shape[0] // CHUNKS
+
+    def guarded(condition, action):
+        if condition is None:
+            action()
+        else:
+            pl.when(condition)(action)
+
+    def both(first, second):
+        if first is None:
+            return second
+        return first if second is None else jnp.logical_and(first, second)
+
+    barrier = pltpu.get_barrier_semaphore()
+    pl.semaphore_signal(barrier, inc=1, device_id={"tp": 1 - tp}, device_id_type=MESH)
+    for way, peer in peers.items():
+        guarded(
+            exists[way],
+            lambda peer=peer: pl.semaphore_signal(
+                barrier, inc=1, device_id={"fs": peer}, device_id_type=MESH
+            ),
+        )
+    along_z = jnp.minimum(z, 1) + jnp.minimum(depth - 1 - z, 1)
+    pl.semaphore_wait(barrier, 3 + along_z)
+
+    sent = []
+
+    def copy_of(matrix, way, block, chunk, own):
+        part = pl.ds(chunk * rows, rows)
+        target = full_refs[matrix].at[block, part]
+        return pltpu.make_async_remote_copy(
+            src_ref=low_refs[matrix].at[part] if own else target,
+            dst_ref=target,
+            send_sem=send_sem.at[matrix, way, block, chunk],
+            recv_sem=recv_sem.at[matrix, block, chunk],
+            device_id={"fs": peers[way]},
+            device_id_type=MESH,
+        )
+
+    def send(matrix, way, block, chunk, own=False, given=None):
+        condition = both(given, exists[way])
+        guarded(condition, lambda: copy_of(matrix, way, block, chunk, own).start())
+        sent.append((condition, matrix, way, block, chunk, own))
+
+    def arrive(matrix, block, chunk, given=None):
+        guarded(given, lambda: copy_of(matrix, ALONG_A, block, chunk, False).wait_recv())
+
+    pair = pltpu.make_async_remote_copy(
+        src_ref=prompt_ref,
+        dst_ref=both_ref.at[tp],
+        send_sem=pair_sem.at[0],
+        recv_sem=pair_sem.at[1],
+        device_id={"tp": 1 - tp},
+        device_id_type=MESH,
+    )
+    chunks = range(CHUNKS)
+    for chunk in chunks:
+        send(UP, ALONG_A, fs, chunk, True)
+        send(DOWN, ALONG_B, fs, chunk, True)
+        send(GATE, Z_UP, fs, chunk, True)
+        send(GATE, Z_DOWN, fs, chunk, True)
+    for matrix in (UP, DOWN):
+        for chunk in chunks:
+            send(matrix, Z_UP, fs, chunk, True)
+            send(matrix, Z_DOWN, fs, chunk, True)
+    for chunk in chunks:
+        send(GATE, ALONG_A, fs, chunk, True)
+        send(GATE, ALONG_B, fs, chunk, True)
+    for chunk in chunks:
+        send(DOWN, ALONG_A, fs, chunk, True)
+        send(UP, ALONG_B, fs, chunk, True)
+    pair.start()
+    local = [
+        pltpu.make_async_copy(low_refs[m], full_refs[m].at[fs], own_sem.at[m]) for m in (GATE, UP, DOWN)
+    ] + [pltpu.make_async_copy(prompt_ref, both_ref.at[tp], own_sem.at[3])]
+    for copy in local:
+        copy.start()
+
+    for chunk in chunks:
+        for matrix, block, last in ((UP, fs + to_a, ALONG_B), (DOWN, fs + to_b, ALONG_A)):
+            arrive(matrix, block, chunk)
+            send(matrix, Z_UP, block, chunk)
+            send(matrix, Z_DOWN, block, chunk)
+            send(matrix, last, block, chunk)
+    for chunk in chunks:
+        arrive(GATE, fs + to_a, chunk)
+        send(GATE, ALONG_B, fs + to_a, chunk)
+    for step in range(1, depth):
+        sides = ((z >= step, fs - 4 * step, Z_UP), (z + step < depth, fs + 4 * step, Z_DOWN))
+        for matrix, offset, lasts in (
+            (GATE, 0, (ALONG_A, ALONG_B)),
+            (UP, 0, (ALONG_B,)),
+            (DOWN, 0, (ALONG_A,)),
+            (UP, to_a, (ALONG_B,)),
+            (DOWN, to_b, (ALONG_A,)),
+        ):
+            for chunk in chunks:
+                for there, block, onward in sides:
+                    arrive(matrix, block + offset, chunk, there)
+                    if step < depth - 1:
+                        send(matrix, onward, block + offset, chunk, given=there)
+                    for way in lasts:
+                        send(matrix, way, block + offset, chunk, given=there)
+        for chunk in chunks:
+            for there, block, _ in sides:
+                arrive(GATE, block + to_a, chunk, there)
+                send(GATE, ALONG_B, block + to_a, chunk, given=there)
+
+    for step in range(depth):
+        sides = ((z >= step, fs - 4 * step), (z + step < depth, fs + 4 * step)) if step else ((None, fs),)
+        for there, block in sides:
+            for chunk in chunks:
+                arrive(GATE, block + to_b, chunk, there)
+                arrive(GATE, block + to_a + to_b, chunk, there)
+                arrive(UP, block + to_b, chunk, there)
+                arrive(UP, block + to_a + to_b, chunk, there)
+                arrive(DOWN, block + to_a, chunk, there)
+                arrive(DOWN, block + to_a + to_b, chunk, there)
+    for condition, matrix, way, block, chunk, own in sent:
+        guarded(condition, lambda: copy_of(matrix, way, block, chunk, own).wait_send())
+    pair.wait()
+    for copy in local:
+        copy.wait()
+
+
+def gather(depth, lows, prompt):
+    blocks = 4 * depth
+    full = jax.ShapeDtypeStruct((blocks,) + lows[0].shape, lows[0].dtype)
+
+    def kernel(g, u, d, p, g_full, u_full, d_full, p_both, *semaphores):
+        gather_kernel(depth, (g, u, d), p, (g_full, u_full, d_full), p_both, *semaphores)
+
+    moved = (blocks - 1) * 3 * lows[0].size * 2
+    return pl.pallas_call(
+        kernel,
+        out_shape=(full, full, full, jax.ShapeDtypeStruct((2,) + prompt.shape, prompt.dtype)),
+        in_specs=[pl.BlockSpec(memory_space=pltpu.VMEM)] * 4,
+        out_specs=[pl.BlockSpec(memory_space=pl.ANY)] * 4,
+        scratch_shapes=[
+            pltpu.SemaphoreType.DMA((3, 4, blocks, CHUNKS)),
+            pltpu.SemaphoreType.DMA((3, blocks, CHUNKS)),
+            pltpu.SemaphoreType.DMA((4,)),
+            pltpu.SemaphoreType.DMA((2,)),
+        ],
+        compiler_params=pltpu.CompilerParams(
+            collective_id=0, has_side_effects=True
+        ),
+        cost_estimate=pl.CostEstimate(flops=0, bytes_accessed=2 * moved, transcendentals=0),
+        name="gather",
+    )(*lows, prompt)
+
+
+def apply_kernel(steps, both_ref, g_ref, u_ref, d_ref, g_out, u_out, d_out, part_ref, normed, gate, up, hidden):
+    k = pl.program_id(0)
+    group, rows, lanes = g_ref.shape
+    width = group * lanes
+
+    def joined(ref):
+        return jnp.concatenate([ref[i] for i in range(group)], axis=1)
+
+    @pl.when(k == 0)
+    def _():
+        halves = [both_ref[i].astype(jnp.float32) for i in range(both_ref.shape[0])]
+        count = sum(half.shape[1] for half in halves)
+        total = sum(jnp.sum(half * half, axis=1, keepdims=True) for half in halves)
+        scale = lax.rsqrt(total / count + 1e-06)
+        values = jnp.concatenate([(half * scale).astype(jnp.bfloat16) for half in halves], axis=1)
+        for i in range(steps):
+            normed[i] = values[:, i * width : (i + 1) * width]
+        gate[...] = jnp.zeros_like(gate)
+        up[...] = jnp.zeros_like(up)
+
+    @pl.when(k < steps)
+    def _():
+        contract = (((1,), (1,)), ((), ()))
+        g, u = joined(g_ref), joined(u_ref)
+        g_out[...] = g
+        u_out[...] = u
+        left = normed[k]
+        gate[...] += lax.dot_general(left, g, contract, preferred_element_type=jnp.float32)
+        up[...] += lax.dot_general(left, u, contract, preferred_element_type=jnp.float32)
+
+    @pl.when(k == steps - 1)
+    def _():
+        value = gate[...]
+        hidden[...] = (value / (1.0 + jnp.exp(-value)) * up[...]).astype(jnp.bfloat16)
+
+    @pl.when(k >= steps)
+    def _():
+        d = joined(d_ref)
+        d_out[...] = d
+        part_ref[...] = jnp.dot(hidden[...], d, preferred_element_type=jnp.float32)
+
+
+def apply(both, g, u, d):
+    blocks, rows, lanes = g.shape
+    tokens = both.shape[1]
+    group = max(n for n in (1, 2, 4) if blocks % n == 0)
+    steps, width = blocks // group, group * lanes
+    early = lambda k: jnp.minimum(k, steps - 1)
+    late = lambda k: jnp.maximum(k - steps, 0)
+    whole = jax.ShapeDtypeStruct((rows, blocks * lanes), g.dtype)
+    return pl.pallas_call(
+        functools.partial(apply_kernel, steps),
+        grid=(2 * steps,),
+        out_shape=(whole, whole, whole, jax.ShapeDtypeStruct((tokens, blocks * lanes), jnp.float32)),
+        in_specs=[
+            pl.BlockSpec(both.shape, lambda k: (0, 0, 0)),
+            pl.BlockSpec((group, rows, lanes), lambda k: (early(k), 0, 0)),
+            pl.BlockSpec((group, rows, lanes), lambda k: (early(k), 0, 0)),
+            pl.BlockSpec((group, rows, lanes), lambda k: (late(k), 0, 0)),
+        ],
+        out_specs=[
+            pl.BlockSpec((rows, width), lambda k: (0, early(k))),
+            pl.BlockSpec((rows, width), lambda k: (0, early(k))),
+            pl.BlockSpec((rows, width), lambda k: (0, late(k))),
+            pl.BlockSpec((tokens, width), lambda k: (0, late(k))),
+        ],
+        scratch_shapes=[
+            pltpu.VMEM((steps, tokens, width), jnp.bfloat16),
+            pltpu.VMEM((tokens, rows), jnp.float32),
+            pltpu.VMEM((tokens, rows), jnp.float32),
+            pltpu.VMEM((tokens, rows), jnp.bfloat16),
+        ],
+        compiler_params=pltpu.CompilerParams(vmem_limit_bytes=56 * 2**20),
+        name="apply",
+    )(both, g, u, d)
+
+
+def sum_kernel(part_ref, mixed_ref, other, send_sem, recv_sem):
+    tp = lax.axis_index("tp")
+    width = other.shape[1]
+    barrier = pltpu.get_barrier_semaphore()
+    pl.semaphore_signal(barrier, inc=1, device_id={"tp": 1 - tp}, device_id_type=MESH)
+    pl.semaphore_wait(barrier, 1)
+    copy = pltpu.make_async_remote_copy(
+        src_ref=part_ref.at[:, pl.ds(pl.multiple_of((1 - tp) * width, LANES), width)],
+        dst_ref=other,
+        send_sem=send_sem,
+        recv_sem=recv_sem,
+        device_id={"tp": 1 - tp},
+        device_id_type=MESH,
+    )
+    copy.start()
+    copy.wait()
+    own = part_ref[:, pl.ds(pl.multiple_of(tp * width, LANES), width)]
+    mixed_ref[...] = (own + other[...]).astype(mixed_ref.dtype)
+
+
+def summed(part):
+    tokens, features = part.shape
+    return pl.pallas_call(
+        sum_kernel,
+        out_shape=jax.ShapeDtypeStruct((tokens, features // 2), jnp.bfloat16),
+        in_specs=[pl.BlockSpec(memory_space=pltpu.VMEM)],
+        out_specs=pl.BlockSpec(memory_space=pltpu.VMEM),
+        scratch_shapes=[
+            pltpu.VMEM((tokens, features // 2), jnp.float32),
+            pltpu.SemaphoreType.DMA,
+            pltpu.SemaphoreType.DMA,
+        ],
+        compiler_params=pltpu.CompilerParams(collective_id=1, has_side_effects=True),
+        name="summed",
+    )(part)
+
+
+def rounded(norm_gain, gate_master, up_master, down_master):
     gain_col = norm_gain[:, None]
-    gate_low = (gate_master * gain_col).astype(jnp.bfloat16).T
-    up_low = (up_master * gain_col).astype(jnp.bfloat16).T
-    down_low = down_master.astype(jnp.bfloat16).T
+    return (
+        (gate_master * gain_col).astype(jnp.bfloat16).T,
+        (up_master * gain_col).astype(jnp.bfloat16).T,
+        down_master.astype(jnp.bfloat16).T,
+    )
+
+
+def by_kernels(depth, prompt, *weights):
+    g, u, d, both = gather(depth, rounded(*weights), prompt)
+    gate_new, up_new, down_new, part = apply(both, g, u, d)
+    return gate_new, up_new, down_new, summed(part).T
+
+
+def by_collectives(prompt, *weights):
+    gate_low, up_low, down_low = rounded(*weights)
     whole = lax.all_gather(prompt, "tp", axis=1, tiled=True)
     values = whole.astype(jnp.float32)
     normed = (values * lax.rsqrt(jnp.mean(values * values, axis=1, keepdims=True) + 1e-06)).astype(
@@ -36,6 +331,14 @@
 
 def solution(mesh):
     placed = (P("fs", "tp"), P("fs"), P("fs", "tp"), P("fs", "tp"), P("fs", "tp"))
+    members, pair = mesh.shape["fs"], mesh.shape["tp"]
+
+    def on_device(prompt, norm_gain, *masters):
+        aligned = norm_gain.shape[0] % LANES == 0 and masters[0].shape[1] % (16 * CHUNKS) == 0
+        if aligned and pair == 2 and members % 4 == 0 and prompt.shape[0] % 16 == 0:
+            return by_kernels(members // 4, prompt, norm_gain, *masters)
+        return by_collectives(prompt, norm_gain, *masters)
+
     return jax.shard_map(
         on_device,
         mesh=mesh,

time: 415 us -> 181 us (0.44)
  waiting for transfers between devices: 365 us -> 0 us
  Pallas kernels: 0 us -> 172 us
  matrix products: 16 us -> 0 us
  between operations: 13.9 us -> 0.66 us
  local copies, waits for them, and re-layouts: 15.2 us -> 6.8 us
    all_gather x4 -> x0, waiting for transfers between devices: 355 us -> none  [the longest x1 118 us: on_device(): lax.all_gather(gate_low, 'fs', axis=1, tiled=True)]
    pallas_call x0 -> x3, Pallas kernels: none -> 172 us  [the longest x1 145 us: gather(): pl.pallas_call(kernel, out_shape=(full, full, full, jax.ShapeDtypeStruct(...]
    dot_general x2 -> x0, matrix products: 16 us -> none  [the longest x1 10.6 us: on_device(): lax.dot_general(down_new, hidden, (((0,), (1,)), ((), ())), preferred_ele...]
    reduce_scatter x1 -> x0, waiting for transfers between devices: 8.65 us -> none  [on_device(): lax.psum_scatter(lax.dot_general(down_new, hidden, (((0,), (1,)), ((), ()...]
    unnamed x22 -> x4, local copies, waits for them, and re-layouts: 15.2 us -> 6.8 us
  transfers between devices with their start and end apart: 5 -> 0, of which waited for: 5 -> 0; matrix products, arithmetic and copies ran while one was open for 3% -> 0% of each run, Pallas kernels for 0% -> 0%
where the time goes in v1:
time: 181 us
  Pallas kernels  172 us (95%)
  local copies, waits for them, and re-layouts  6.8 us (4%)
    pallas_call x1, Pallas kernels, gather(): pl.pallas_call(kernel, out_shape=(full, full, full, jax.ShapeDtypeStruct(...  145 us
    pallas_call x1, Pallas kernels, apply(): pl.pallas_call(functools.partial(apply_kernel, steps), grid=(2 * steps,),...  20.5 us
    unnamed x4, local copies, waits for them, and re-layouts  6.8 us
    pallas_call x1, Pallas kernels, summed(): pl.pallas_call(sum_kernel, out_shape=jax.ShapeDtypeStruct((tokens, featur...  5.9 us

profile of v1, /device:TPU:0, one launch (start us, length us, event | category | flops | bytes accessed | tf_op | source)
XLA Modules:
  0.0 181.0 jit_solution(16303001254275431046)
XLA Ops:
  0.6 2.0 %copy.11 = bf16[128,1536]{0,1:T(8,128)(2,1)} copy(f32[128,1536]{1,0:T(8,128)} %param.9) | data formatting | bytes 1179648 | tf_op args[4]
  2.7 1.4 copy.9
  4.1 1.4 copy.10
  5.5 1.7 fusion.1
  7.1 145.5 %gather.1 = (bf16[16,1536,128]{2,1,0:T(8,128)(2,1)}, bf16[16,1536,128]{2,1,0:T(8,128)(2,1)}, bf16[16,1536,128]{2,1,0:T(8,128)(2,1)}, bf16[2,320,1024]{2,1,0:T(8,128)(2,1)}) custom-call(bf16[1536,128]{1,0:T(8,128)(2,1)} %get-tuple-element.21.g, bf16[1536,128]{1,0:T(8,128)(2,1)} %get-tuple-element.20.u, bf16[1536,128]{1,0:T(8,128)(2,1)} %bitcast.9, ...), custom_call_target="tpu_custom_call" | custom-call | bytes 35389440 | tf_op jit(solution)/shard_map/gather/pallas_call | solution.py:157
  152.6 20.5 %apply.1 = (bf16[1536,2048]{1,0:T(8,128)(2,1)}, bf16[1536,2048]{1,0:T(8,128)(2,1)}, bf16[1536,2048]{1,0:T(8,128)(2,1)}, f32[320,2048]{1,0:T(8,128)}) custom-call(bf16[2,320,1024]{2,1,0:T(8,128)(2,1)} %get-tuple-element.12.both_ref, bf16[16,1536,128]{2,1,0:T(8,128)(2,1)} %get-tuple-element.13.g_ref, bf16[16,1536,128]{2,1,0:T(8,128)(2,1)} %get-tuple-element.14.u_ref, ...), custom_call_target="tpu_custom_call" | custom-call | tf_op jit(solution)/shard_map/apply/pallas_call | solution.py:226
  173.1 5.9 %summed.1 = bf16[320,1024]{1,0:T(8,128)(2,1)} custom-call(f32[320,2048]{1,0:T(8,128)} %get-tuple-element.19.part_ref), custom_call_target="tpu_custom_call" | custom-call | tf_op jit(solution)/shard_map/summed/pallas_call | solution.py:275
  179.0 2.0 %copy.13 = bf16[1024,320]{0,1:T(8,128)(2,1)} copy(bf16[1024,320]{0,1:T(8,128)(2,1)} %bitcast.8) | data formatting | bytes 1310720

commit v2 on v1

--- a/solution.py
+++ b/solution.py
@@ -14,7 +14,7 @@
 CHUNKS = 2
 
 
-def gather_kernel(depth, low_refs, prompt_ref, full_refs, both_ref, send_sem, recv_sem, own_sem, pair_sem):
+def gather_kernel(depth, low_refs, prompt_ref, full_refs, both_ref, send_sem, recv_sem, pair_sem):
     fs, tp = lax.axis_index("fs"), lax.axis_index("tp")
     z, y, x = fs // 4, lax.rem(fs // 2, 2), lax.rem(fs, 2)
     at_a, at_b = x * (1 - tp) + y * tp, y * (1 - tp) + x * tp
@@ -93,11 +93,9 @@
         send(DOWN, ALONG_A, fs, chunk, True)
         send(UP, ALONG_B, fs, chunk, True)
     pair.start()
-    local = [
-        pltpu.make_async_copy(low_refs[m], full_refs[m].at[fs], own_sem.at[m]) for m in (GATE, UP, DOWN)
-    ] + [pltpu.make_async_copy(prompt_ref, both_ref.at[tp], own_sem.at[3])]
-    for copy in local:
-        copy.start()
+    for low, full in zip(low_refs, full_refs):
+        full[fs] = low[...]
+    both_ref[tp] = prompt_ref[...]
 
     for chunk in chunks:
         for matrix, block, last in ((UP, fs + to_a, ALONG_B), (DOWN, fs + to_b, ALONG_A)):
@@ -142,13 +140,11 @@
     for condition, matrix, way, block, chunk, own in sent:
         guarded(condition, lambda: copy_of(matrix, way, block, chunk, own).wait_send())
     pair.wait()
-    for copy in local:
-        copy.wait()
 
 
 def gather(depth, lows, prompt):
     blocks = 4 * depth
-    full = jax.ShapeDtypeStruct((blocks,) + lows[0].shape, lows[0].dtype)
+    full = pltpu.VMEM((blocks,) + lows[0].shape, lows[0].dtype)
 
     def kernel(g, u, d, p, g_full, u_full, d_full, p_both, *semaphores):
         gather_kernel(depth, (g, u, d), p, (g_full, u_full, d_full), p_both, *semaphores)
@@ -156,17 +152,16 @@
     moved = (blocks - 1) * 3 * lows[0].size * 2
     return pl.pallas_call(
         kernel,
-        out_shape=(full, full, full, jax.ShapeDtypeStruct((2,) + prompt.shape, prompt.dtype)),
+        out_shape=(full, full, full, pltpu.VMEM((2,) + prompt.shape, prompt.dtype)),
         in_specs=[pl.BlockSpec(memory_space=pltpu.VMEM)] * 4,
-        out_specs=[pl.BlockSpec(memory_space=pl.ANY)] * 4,
+        out_specs=[pl.BlockSpec(memory_space=pltpu.VMEM)] * 4,
         scratch_shapes=[
             pltpu.SemaphoreType.DMA((3, 4, blocks, CHUNKS)),
             pltpu.SemaphoreType.DMA((3, blocks, CHUNKS)),
-            pltpu.SemaphoreType.DMA((4,)),
             pltpu.SemaphoreType.DMA((2,)),
         ],
         compiler_params=pltpu.CompilerParams(
-            collective_id=0, has_side_effects=True
+            collective_id=0, has_side_effects=True, vmem_limit_bytes=26 * 2**20
         ),
         cost_estimate=pl.CostEstimate(flops=0, bytes_accessed=2 * moved, transcendentals=0),
         name="gather",
@@ -175,11 +170,11 @@
 
 def apply_kernel(steps, both_ref, g_ref, u_ref, d_ref, g_out, u_out, d_out, part_ref, normed, gate, up, hidden):
     k = pl.program_id(0)
-    group, rows, lanes = g_ref.shape
-    width = group * lanes
-
-    def joined(ref):
-        return jnp.concatenate([ref[i] for i in range(group)], axis=1)
+    group = g_ref.shape[0] // steps
+    width = group * g_ref.shape[2]
+
+    def joined(ref, first):
+        return jnp.concatenate([ref[first * group + i] for i in range(group)], axis=1)
 
     @pl.when(k == 0)
     def _():
@@ -196,7 +191,7 @@
     @pl.when(k < steps)
     def _():
         contract = (((1,), (1,)), ((), ()))
-        g, u = joined(g_ref), joined(u_ref)
+        g, u = joined(g_ref, k), joined(u_ref, k)
         g_out[...] = g
         u_out[...] = u
         left = normed[k]
@@ -210,7 +205,7 @@
 
     @pl.when(k >= steps)
     def _():
-        d = joined(d_ref)
+        d = joined(d_ref, k - steps)
         d_out[...] = d
         part_ref[...] = jnp.dot(hidden[...], d, preferred_element_type=jnp.float32)
 
@@ -228,10 +223,10 @@
         grid=(2 * steps,),
         out_shape=(whole, whole, whole, jax.ShapeDtypeStruct((tokens, blocks * lanes), jnp.float32)),
         in_specs=[
-            pl.BlockSpec(both.shape, lambda k: (0, 0, 0)),
-            pl.BlockSpec((group, rows, lanes), lambda k: (early(k), 0, 0)),
-            pl.BlockSpec((group, rows, lanes), lambda k: (early(k), 0, 0)),
-            pl.BlockSpec((group, rows, lanes), lambda k: (late(k), 0, 0)),
+            pl.BlockSpec(memory_space=pltpu.VMEM),
+            pl.BlockSpec(memory_space=pltpu.VMEM),
+            pl.BlockSpec(memory_space=pltpu.VMEM),
+            pl.BlockSpec(memory_space=pltpu.VMEM),
         ],
         out_specs=[
             pl.BlockSpec((rows, width), lambda k: (0, early(k))),
@@ -245,7 +240,7 @@
             pltpu.VMEM((tokens, rows), jnp.float32),
             pltpu.VMEM((tokens, rows), jnp.bfloat16),
         ],
-        compiler_params=pltpu.CompilerParams(vmem_limit_bytes=56 * 2**20),
+        compiler_params=pltpu.CompilerParams(vmem_limit_bytes=32 * 2**20),
         name="apply",
     )(both, g, u, d)
 
@@ -282,7 +277,7 @@
             pltpu.SemaphoreType.DMA,
             pltpu.SemaphoreType.DMA,
         ],
-        compiler_params=pltpu.CompilerParams(collective_id=1, has_side_effects=True),
+        compiler_params=pltpu.CompilerParams(collective_id=1, has_side_effects=True, vmem_limit_bytes=12 * 2**20),
         name="summed",
     )(part)
 
@@ -296,8 +291,31 @@
     )
 
 
+def round_kernel(gain_ref, g_ref, u_ref, d_ref, g_out, u_out, d_out):
+    gain = gain_ref[...]
+    g_out[...] = (g_ref[...] * gain).T.astype(g_out.dtype)
+    u_out[...] = (u_ref[...] * gain).T.astype(u_out.dtype)
+    d_out[...] = d_ref[...].T.astype(d_out.dtype)
+
+
+def rounded_by_kernel(norm_gain, *masters):
+    features, rows = masters[0].shape
+    width = max(n for n in (LANES, 2 * LANES, 4 * LANES) if rows % n == 0)
+    low = jax.ShapeDtypeStruct((rows, features), jnp.bfloat16)
+    return pl.pallas_call(
+        round_kernel,
+        grid=(rows // width,),
+        out_shape=(low,) * 3,
+        in_specs=[pl.BlockSpec((features, 1), lambda k: (0, 0))]
+        + [pl.BlockSpec((features, width), lambda k: (0, k))] * 3,
+        out_specs=[pl.BlockSpec((width, features), lambda k: (k, 0))] * 3,
+        compiler_params=pltpu.CompilerParams(vmem_limit_bytes=8 * 2**20),
+        name="rounded",
+    )(norm_gain[:, None], *masters)
+
+
 def by_kernels(depth, prompt, *weights):
-    g, u, d, both = gather(depth, rounded(*weights), prompt)
+    g, u, d, both = gather(depth, rounded_by_kernel(*weights), prompt)
     gate_new, up_new, down_new, part = apply(both, g, u, d)
     return gate_new, up_new, down_new, summed(part).T
 
@@ -334,7 +352,7 @@
     members, pair = mesh.shape["fs"], mesh.shape["tp"]
 
     def on_device(prompt, norm_gain, *masters):
-        aligned = norm_gain.shape[0] % LANES == 0 and masters[0].shape[1] % (16 * CHUNKS) == 0
+        aligned = norm_gain.shape[0] % LANES == 0 and masters[0].shape[1] % LANES == 0
         if aligned and pair == 2 and members % 4 == 0 and prompt.shape[0] % 16 == 0:
             return by_kernels(members // 4, prompt, norm_gain, *masters)
         return by_collectives(prompt, norm_gain, *masters)

time: 181 us -> 167 us (0.923)
  Pallas kernels: 172 us -> 160 us
    pallas_call x1, Pallas kernels: 20.5 us -> 12.2 us  [apply(): pl.pallas_call(functools.partial(apply_kernel, steps), grid=(2 * steps,),...]
    pallas_call x1, Pallas kernels: 5.9 us -> 3.32 us  [summed(): pl.pallas_call(sum_kernel, out_shape=jax.ShapeDtypeStruct((tokens, featur...]
    unnamed x4 -> x9, local copies, waits for them, and re-layouts: 6.8 us -> 5.32 us
    pallas_call x1 -> x2, Pallas kernels: 145 us -> 145 us  [the longest x1 144 us: gather(): pl.pallas_call(kernel, out_shape=(full, full, full, pltpu.VMEM((2,) + pro...]
where the time goes in v2:
time: 167 us
  Pallas kernels  160 us (96%)
  local copies, waits for them, and re-layouts  6.08 us (4%)
    pallas_call x1, Pallas kernels, gather(): pl.pallas_call(kernel, out_shape=(full, full, full, pltpu.VMEM((2,) + pro...  144 us
    pallas_call x1, Pallas kernels, apply(): pl.pallas_call(functools.partial(apply_kernel, steps), grid=(2 * steps,),...  12.2 us
    unnamed x9, local copies, waits for them, and re-layouts  5.32 us

profile of v2, /device:TPU:0, one launch (start us, length us, event | category | flops | bytes accessed | tf_op | source)
XLA Modules:
  0.0 166.8 jit_solution(8548270689838953330)
XLA Ops:
  0.6 0.8 copy.9.gain_ref
  1.4 0.0 copy-start
  1.4 1.1 copy-done
  2.5 0.0 copy-start.1
  2.5 1.1 copy-done.1
  3.7 0.0 copy-start.2
  3.7 1.1 copy-done.2
  4.8 0.9 rounded.1
  5.7 0.0 copy-start.3
  5.7 1.1 copy-done.3
  6.8 143.6 %gather.1 = (bf16[16,1536,128]{2,1,0:T(8,128)(2,1)S(1)}, bf16[16,1536,128]{2,1,0:T(8,128)(2,1)S(1)}, bf16[16,1536,128]{2,1,0:T(8,128)(2,1)S(1)}, bf16[2,320,1024]{2,1,0:T(8,128)(2,1)S(1)}) custom-call(bf16[1536,128]{1,0:T(8,128)(2,1)S(1)} %get-tuple-element.15.g, bf16[1536,128]{1,0:T(8,128)(2,1)S(1)} %get-tuple-element.16.u, ...), custom_call_target="tpu_custom_call" | custom-call | bytes 35389440 | tf_op jit(solution)/shard_map/gather/pallas_call | solution.py:153
  150.4 12.2 %apply.1 = (bf16[1536,2048]{1,0:T(8,128)(2,1)}, bf16[1536,2048]{1,0:T(8,128)(2,1)}, bf16[1536,2048]{1,0:T(8,128)(2,1)}, f32[320,2048]{1,0:T(8,128)S(1)}) custom-call(bf16[2,320,1024]{2,1,0:T(8,128)(2,1)S(1)} %get-tuple-element.18.both_ref, bf16[16,1536,128]{2,1,0:T(8,128)(2,1)S(1)} %get-tuple-element.19.g_ref, ...), custom_call_target="tpu_custom_call" | custom-call | tf_op jit(solution)/shard_map/apply/pallas_call | solution.py:221
  162.6 3.3 %summed.1 = bf16[320,1024]{1,0:T(8,128)(2,1)S(1)} custom-call(f32[320,2048]{1,0:T(8,128)S(1)} %get-tuple-element.25.part_ref), custom_call_target="tpu_custom_call" | custom-call | tf_op jit(solution)/shard_map/summed/pallas_call | solution.py:270
  166.0 0.8 copy.11
Async XLA Ops:
  1.4 1.1 copy-start
  2.5 1.1 copy-start.1
  3.7 1.1 copy-start.2
  5.7 1.1 copy-start.3

commit v3 on v2

--- a/solution.py
+++ b/solution.py
@@ -11,7 +11,7 @@
 LANES = 128
 GATE, UP, DOWN = 0, 1, 2
 Z_UP, Z_DOWN, ALONG_A, ALONG_B = 0, 1, 2, 3
-CHUNKS = 2
+CHUNKS = 4
 
 
 def gather_kernel(depth, low_refs, prompt_ref, full_refs, both_ref, send_sem, recv_sem, pair_sem):
@@ -291,27 +291,36 @@
     )
 
 
-def round_kernel(gain_ref, g_ref, u_ref, d_ref, g_out, u_out, d_out):
+def round_kernel(gain_ref, g_ref, u_ref, d_ref, g_out, u_out, d_out, held, sems):
+    copies = [
+        pltpu.make_async_copy(ref, held.at[i], sems.at[i]) for i, ref in enumerate((g_ref, u_ref, d_ref))
+    ]
+    for copy in copies:
+        copy.start()
     gain = gain_ref[...]
-    g_out[...] = (g_ref[...] * gain).T.astype(g_out.dtype)
-    u_out[...] = (u_ref[...] * gain).T.astype(u_out.dtype)
-    d_out[...] = d_ref[...].T.astype(d_out.dtype)
+    copies[0].wait()
+    g_out[...] = (held[0].T * gain).astype(g_out.dtype)
+    copies[1].wait()
+    u_out[...] = (held[1].T * gain).astype(u_out.dtype)
+    copies[2].wait()
+    d_out[...] = held[2].T.astype(d_out.dtype)
 
 
 def rounded_by_kernel(norm_gain, *masters):
     features, rows = masters[0].shape
-    width = max(n for n in (LANES, 2 * LANES, 4 * LANES) if rows % n == 0)
-    low = jax.ShapeDtypeStruct((rows, features), jnp.bfloat16)
+    low = pltpu.VMEM((rows, features), jnp.bfloat16)
     return pl.pallas_call(
         round_kernel,
-        grid=(rows // width,),
         out_shape=(low,) * 3,
-        in_specs=[pl.BlockSpec((features, 1), lambda k: (0, 0))]
-        + [pl.BlockSpec((features, width), lambda k: (0, k))] * 3,
-        out_specs=[pl.BlockSpec((width, features), lambda k: (k, 0))] * 3,
-        compiler_params=pltpu.CompilerParams(vmem_limit_bytes=8 * 2**20),
+        in_specs=[pl.BlockSpec(memory_space=pltpu.VMEM)] + [pl.BlockSpec(memory_space=pltpu.HBM)] * 3,
+        out_specs=[pl.BlockSpec(memory_space=pltpu.VMEM)] * 3,
+        scratch_shapes=[
+            pltpu.VMEM((3, features, rows), jnp.float32),
+            pltpu.SemaphoreType.DMA((3,)),
+        ],
+        compiler_params=pltpu.CompilerParams(vmem_limit_bytes=61 * 2**20),
         name="rounded",
-    )(norm_gain[:, None], *masters)
+    )(norm_gain[None, :], *masters)
 
 
 def by_kernels(depth, prompt, *weights):

time: 167 us -> 168 us (level)
  Pallas kernels: 160 us -> 166 us
  local copies, waits for them, and re-layouts: 6.08 us -> 1.92 us
    pallas_call x1, Pallas kernels: 144 us -> 148 us  [gather(): pl.pallas_call(kernel, out_shape=(full, full, full, pltpu.VMEM((2,) + pro...]
    unnamed x9 -> x3, local copies, waits for them, and re-layouts: 5.32 us -> 1.92 us
where the time goes in v3:
time: 168 us
  Pallas kernels  166 us (99%)
  local copies, waits for them, and re-layouts  1.92 us (1%)
    pallas_call x1, Pallas kernels, gather(): pl.pallas_call(kernel, out_shape=(full, full, full, pltpu.VMEM((2,) + pro...  148 us
    pallas_call x1, Pallas kernels, apply(): pl.pallas_call(functools.partial(apply_kernel, steps), grid=(2 * steps,),...  12.2 us

profile of v3, /device:TPU:0, one launch (start us, length us, event | category | flops | bytes accessed | tf_op | source)
XLA Modules:
  0.0 168.2 jit_solution(5671676204019989263)
XLA Ops:
  0.6 2.5 %rounded.1 = (bf16[1536,128]{1,0:T(8,128)(2,1)S(1)}, bf16[1536,128]{1,0:T(8,128)(2,1)S(1)}, bf16[1536,128]{1,0:T(8,128)(2,1)S(1)}) custom-call(f32[1,128]{1,0:T(1,128)} %bitcast.3, f32[128,1536]{1,0:T(8,128)} %g_ref.1, f32[128,1536]{1,0:T(8,128)} %u_ref.1, f32[128,1536]{1,0:T(8,128)} %d_ref.1), custom_call_target="tpu_custom_call" | custom-call | tf_op jit(solution)/shard_map/rounded/pallas_call | solution.py:312
  3.2 0.0 copy-start
  3.2 1.1 copy-done
  4.3 147.7 %gather.1 = (bf16[16,1536,128]{2,1,0:T(8,128)(2,1)S(1)}, bf16[16,1536,128]{2,1,0:T(8,128)(2,1)S(1)}, bf16[16,1536,128]{2,1,0:T(8,128)(2,1)S(1)}, bf16[2,320,1024]{2,1,0:T(8,128)(2,1)S(1)}) custom-call(bf16[1536,128]{1,0:T(8,128)(2,1)S(1)} %get-tuple-element.15.g, bf16[1536,128]{1,0:T(8,128)(2,1)S(1)} %get-tuple-element.16.u, ...), custom_call_target="tpu_custom_call" | custom-call | bytes 35389440 | tf_op jit(solution)/shard_map/gather/pallas_call | solution.py:153
  151.9 12.2 %apply.1 = (bf16[1536,2048]{1,0:T(8,128)(2,1)}, bf16[1536,2048]{1,0:T(8,128)(2,1)}, bf16[1536,2048]{1,0:T(8,128)(2,1)}, f32[320,2048]{1,0:T(8,128)S(1)}) custom-call(bf16[2,320,1024]{2,1,0:T(8,128)(2,1)S(1)} %get-tuple-element.18.both_ref, bf16[16,1536,128]{2,1,0:T(8,128)(2,1)S(1)} %get-tuple-element.19.g_ref, ...), custom_call_target="tpu_custom_call" | custom-call | tf_op jit(solution)/shard_map/apply/pallas_call | solution.py:221
  164.2 3.2 %summed.1 = bf16[320,1024]{1,0:T(8,128)(2,1)S(1)} custom-call(f32[320,2048]{1,0:T(8,128)S(1)} %get-tuple-element.25.part_ref), custom_call_target="tpu_custom_call" | custom-call | tf_op jit(solution)/shard_map/summed/pallas_call | solution.py:270
  167.3 0.8 copy.10
Async XLA Ops:
  3.2 1.1 copy-start
